TPU v7x, 32 devices: a whole 2x2x4 slice. The times are simulated.
32 devices in a mesh: kv: 8 (over z, y), tp: 4 (over x, core).
Axes of the slice: x: 2, y: 2, z: 4, core: 2. Of those that a mesh axis runs over, the one named last changes fastest.
Arguments:
- tokens: bfloat16 [32, 4096], P(None, ('kv', 'tp')), may hold values from -36 to 36
- first_gain: float32 [4096], P('kv'), may hold values from 0.1 to 1.9
- first_gate: bfloat16 [4096, 11264], P('kv', 'tp'), may hold values from -0.09375 to 0.09375
- first_up: bfloat16 [4096, 11264], P('kv', 'tp'), may hold values from -0.09375 to 0.09375
- first_down: bfloat16 [11264, 4096], P('tp', 'kv'), may hold values from -0.0546875 to 0.0546875
- mix_gain: float32 [4096], P('kv'), may hold values from 0.1 to 1.9
- w_query: bfloat16 [4096, 2048], P('kv', 'tp'), may hold values from -0.09375 to 0.09375
- key_cache: bfloat16 [32, 8192, 1024], P(None, 'kv', 'tp'), may hold values from -100 to 100
- value_cache: bfloat16 [32, 8192, 1024], P(None, 'kv', 'tp'), may hold values from -6 to 6
- map_weight: float32 [32], P('tp'), may hold values from 0.3 to 0.8
- head_gain: float32 [64], replicated, may hold values from 0.1 to 1.9
- w_out: bfloat16 [2048, 4096], P('tp', 'kv'), may hold values from -0.125 to 0.125
- second_gain: float32 [4096], P('kv'), may hold values from 0.1 to 1.9
- second_gate: bfloat16 [4096, 11264], P('kv', 'tp'), may hold values from -0.09375 to 0.09375
- second_up: bfloat16 [4096, 11264], P('kv', 'tp'), may hold values from -0.09375 to 0.09375
- second_down: bfloat16 [11264, 4096], P('tp', 'kv'), may hold values from -0.0546875 to 0.0546875
Outputs:
- mixed: bfloat16 [32, 4096], P(None, ('kv', 'tp'))
All inputs are finite; a program needn't handle non-finite values.
Results may differ from a plain program's by a relative error of at most 0.0158.
Values may be sent and summed in bfloat16 or wider, within the bound.
A program may use at most 128 MiB of HBM per device.

v0:
```python
import math
import jax
import jax.numpy as jnp
from jax import lax
from jax.sharding import PartitionSpec as P

D = 4096
HEAD = 64
EPS = 1e-06
HEAD_SCALE = 0.8


def merged(value, axis, join):
    pieces = jax.tree.map(lambda part: lax.all_gather(part, axis), value)
    head = jax.tree.map(lambda part: part[0], pieces)
    tail = jax.tree.map(lambda part: part[1:], pieces)
    subtotal, _ = lax.scan(lambda subtotal, piece: (join(subtotal, piece), None), head, tail)
    return subtotal


def norm_total(squares):
    return lax.psum(squares, "kv")


def channel_mixer(residual, gain, w_gate, w_up, w_down):
    squares = jnp.sum(residual * residual, axis=1, keepdims=True)
    scaled = (residual * gain).astype(jnp.bfloat16)
    part_gate = jnp.dot(scaled, w_gate, preferred_element_type=jnp.float32)
    part_up = jnp.dot(scaled, w_up, preferred_element_type=jnp.float32)
    row_total = norm_total(squares)
    gate_sum, up_sum = lax.psum((part_gate, part_up), "kv")
    factor = lax.rsqrt(row_total / D + EPS)
    active = (jax.nn.silu(gate_sum * factor) * (up_sum * factor)).astype(jnp.bfloat16)
    partial_value = jnp.dot(active, w_down, preferred_element_type=jnp.float32)
    return lax.psum(partial_value, "tp")


def merge_pair(first, second):
    row_peak = jnp.maximum(first[0], second[0])
    scale_first = jnp.exp(first[0] - row_peak)
    scale_second = jnp.exp(second[0] - row_peak)
    return (
        row_peak,
        first[1] * scale_first + second[1] * scale_second,
        first[2] * scale_first[..., None] + second[2] * scale_second[..., None],
    )


def combine_maps(earlier, later):
    return merge_pair(earlier[:3], later[:3]) + merge_pair(earlier[3:], later[3:])


def attention_mix(
    residual, mix_gain, w_query, key_cache, value_cache, map_weight, head_gain, w_out
):
    squares = jnp.sum(residual * residual, axis=1, keepdims=True)
    scaled = (residual * mix_gain).astype(jnp.bfloat16)
    part_query = jnp.dot(scaled, w_query, preferred_element_type=jnp.float32)
    row_total = norm_total(squares)
    queries = lax.psum(part_query, "kv")
    queries = (queries * lax.rsqrt(row_total / D + EPS)).astype(jnp.bfloat16)
    batch_rows = queries.shape[0]
    kv_local = key_cache.shape[2] // HEAD
    group = queries.shape[1] // (kv_local * HEAD)
    queries = queries.reshape(batch_rows, kv_local, group, HEAD)
    cached = key_cache.reshape(batch_rows, -1, kv_local, HEAD)
    stored = value_cache.reshape(batch_rows, -1, kv_local, HEAD)

    def partial_map(first_col, last_col):
        scores = jnp.einsum(
            "bkgd,bpkd->bkgp",
            queries[..., first_col:last_col],
            cached[..., first_col:last_col],
            preferred_element_type=jnp.float32,
        ) / math.sqrt(last_col - first_col)
        row_peak = jnp.max(scores, axis=3)
        exp_terms = jnp.exp(scores - row_peak[..., None])
        weights_sum = jnp.sum(exp_terms, axis=3)
        summed = jnp.einsum(
            "bkgp,bpkd->bkgd",
            exp_terms.astype(jnp.bfloat16),
            stored,
            preferred_element_type=jnp.float32,
        )
        return (row_peak, weights_sum, summed)

    half_dim = HEAD // 2
    peak_one, sum_one, out_one = partial_map(0, half_dim)
    peak_two, sum_two, out_two = partial_map(half_dim, HEAD)
    peak_one, sum_one, out_one, peak_two, sum_two, out_two = merged(
        (peak_one, sum_one, out_one, peak_two, sum_two, out_two), "kv", combine_maps
    )
    weight = map_weight.reshape(kv_local, group)
    combined = out_one / sum_one[..., None] - weight[..., None] * out_two / sum_two[..., None]
    normed = (
        combined
        * lax.rsqrt(jnp.mean(combined * combined, axis=3, keepdims=True) + EPS)
        * head_gain
        * HEAD_SCALE
    )
    normed = normed.astype(jnp.bfloat16).reshape(batch_rows, kv_local * group * HEAD)
    partial_value = jnp.dot(normed, w_out, preferred_element_type=jnp.float32)
    return lax.psum(partial_value, "tp")


def on_device(
    tokens,
    first_gain,
    first_gate,
    first_up,
    first_down,
    mix_gain,
    w_query,
    key_cache,
    value_cache,
    map_weight,
    head_gain,
    w_out,
    second_gain,
    second_gate,
    second_up,
    second_down,
):
    residual = lax.all_gather(tokens, "tp", axis=1, tiled=True).astype(jnp.float32)
    residual = residual + 0.5 * channel_mixer(
        residual, first_gain, first_gate, first_up, first_down
    )
    residual = residual + attention_mix(
        residual, mix_gain, w_query, key_cache, value_cache, map_weight, head_gain, w_out
    )
    residual = residual + 0.5 * channel_mixer(
        residual, second_gain, second_gate, second_up, second_down
    )
    width = residual.shape[1] // lax.axis_size("tp")
    return lax.dynamic_slice_in_dim(residual, lax.axis_index("tp") * width, width, 1).astype(
        jnp.bfloat16
    )


def solution(mesh):
    placed = (
        P(None, ("kv", "tp")),
        P("kv"),
        P("kv", "tp"),
        P("kv", "tp"),
        P("tp", "kv"),
        P("kv"),
        P("kv", "tp"),
        P(None, "kv", "tp"),
        P(None, "kv", "tp"),
        P("tp"),
        P(),
        P("tp", "kv"),
        P("kv"),
        P("kv", "tp"),
        P("kv", "tp"),
        P("tp", "kv"),
    )
    return jax.shard_map(
        on_device, mesh=mesh, in_specs=placed, out_specs=P(None, ("kv", "tp")), check_vma=False
    )
```

profile of v0, /device:TPU:0, one launch (start us, length us, event | category | flops | bytes accessed | tf_op | source)
XLA Modules:
  0.0 626.8 jit_solution(4104942960489870407)
XLA Ops:
  6.5 6.5 %all_gather.39 = bf16[32,512]{1,0:T(8,128)(2,1)S(1)} all-gather(bf16[32,128]{1,0:T(8,128)(2,1)} %param.18), channel_id=1, replica_groups=mesh['kv'=8,'tp'=4] {'tp'}, dimensions={1}, use_global_device_ids=true | all-gather | bytes 40960 | tf_op jit(solution)/shard_map/all_gather | solution.py:124
  13.0 2.0 fusion.40
  15.0 1.4 fusion.42
  16.6 22.7 %psum.78 = f32[32,1]{0,1:T(1,128)S(1)} all-reduce(f32[32,1]{0,1:T(1,128)S(1)} %bitcast.79), channel_id=1, replica_groups=mesh['kv'=8,'tp'=4] {'kv'}, use_global_device_ids=true, to_apply=%region_2.0 | all-reduce | flops 32 | bytes 256 | tf_op jit(solution)/shard_map/psum | solution.py:22
  39.3 53.8 %all-reduce.19.cloned.1.call-done = (f32[32,2816]{1,0:T(8,128)}, f32[32,2816]{1,0:T(8,128)}) async-done(((f32[32,2816]{1,0:T(8,128)}, f32[32,2816]{1,0:T(8,128)}), (f32[32,2816]{1,0:T(8,128)}, f32[32,2816]{1,0:T(8,128)})) %all-reduce.19.cloned.1.call-update) | async-done | bytes 720912 | tf_op jit(solution)/shard_map/psum | solution.py:31
  93.1 2.4 fusion.28
  95.6 22.5 %copy.107 = bf16[32,1024,256]{1,2,0:T(8,128)(2,1)} copy(bf16[32,1024,256]{2,1,0:T(8,128)(2,1)} %param.25) | data formatting | bytes 33554432 | tf_op args[7]
  118.2 22.6 %copy.110 = bf16[32,1024,256]{1,2,0:T(8,128)(2,1)} copy(bf16[32,1024,256]{2,1,0:T(8,128)(2,1)} %param.26) | data formatting | bytes 33554432 | tf_op args[8]
  140.8 1.0 multiply_reduce_fusion.2
  141.7 19.6 %psum.82 = f32[32,1]{0,1:T(1,128)S(1)} all-reduce(f32[32,1]{0,1:T(1,128)S(1)} %bitcast.80), channel_id=1, replica_groups=mesh['kv'=8,'tp'=4] {'kv'}, use_global_device_ids=true, to_apply=%region_7.8 | all-reduce | flops 32 | bytes 256 | tf_op jit(solution)/shard_map/psum | solution.py:22
  161.3 1.7 fusion.38
  163.1 66.6 %all-reduce.11.cloned.1.call-done = f32[32,512]{1,0:T(8,128)} async-done(((f32[32,512]{1,0:T(8,128)}), f32[32,512]{1,0:T(8,128)}) %all-reduce.11.cloned.1.call-update) | async-done | bytes 65552 | tf_op jit(solution)/shard_map/psum | solution.py:60
  229.6 0.9 multiply_convert_fusion.6
  230.7 4.9 fusion.55
  235.6 4.9 fusion.54
  240.8 0.9 fusion.19
  242.0 30.9 %all-gather.1 = f32[256,4,2]{1,2,0:T(2,128)S(1)} all-gather(f32[32,4,2]{1,2,0:T(2,128)S(1)} %copy.109), channel_id=3, replica_groups=mesh['kv'=8,'tp'=4] {'kv'}, dimensions={0}, use_global_device_ids=true | all-gather | bytes 9216 | tf_op jit(solution)/shard_map/all_gather | solution.py:14
  273.2 1.0 fusion.21
  274.5 30.9 %all-gather.4 = f32[256,4,2]{1,2,0:T(2,128)S(1)} all-gather(f32[32,4,2]{1,2,0:T(2,128)S(1)} %copy.113), channel_id=6, replica_groups=mesh['kv'=8,'tp'=4] {'kv'}, dimensions={0}, use_global_device_ids=true | all-gather | bytes 9216 | tf_op jit(solution)/shard_map/all_gather | solution.py:14
  305.4 31.0 %all-gather = f32[256,4,2]{1,2,0:T(2,128)S(1)} all-gather(f32[32,4,2]{1,2,0:T(2,128)S(1)} %copy.108), channel_id=2, replica_groups=mesh['kv'=8,'tp'=4] {'kv'}, dimensions={0}, use_global_device_ids=true | all-gather | bytes 9216 | tf_op jit(solution)/shard_map/all_gather | solution.py:14
  337.1 31.1 %all-gather.3 = f32[256,4,2]{1,2,0:T(2,128)S(1)} all-gather(f32[32,4,2]{1,2,0:T(2,128)S(1)} %copy.112), channel_id=5, replica_groups=mesh['kv'=8,'tp'=4] {'kv'}, dimensions={0}, use_global_device_ids=true | all-gather | bytes 9216 | tf_op jit(solution)/shard_map/all_gather | solution.py:14
  368.2 0.8 slice.89
  369.0 8.8 %fusion.22 = f32[32,4,2,64]{3,2,1,0:T(2,128)} fusion(bf16[32,1024,4,64]{1,3,2,0:T(8,128)(2,1)} %bitcast.68, f32[32,4,2,1024]{3,2,1,0:T(2,128)S(1)} %get-tuple-element.178, f32[32,4,2]{2,1,0:T(4,128)S(1)} %get-tuple-element.177), kind=kOutput, calls=%fused_computation.32 | convolution fusion | flops 34078720 | bytes 17892352 | tf_op jit(solution)/shard_map/bkgp,bpkd->bkgd/dot_general | solution.py:79
  377.8 8.2 %fusion.24 = f32[32,4,2,64]{3,2,1,0:T(2,128)S(1)} fusion(bf16[32,1024,4,64]{1,3,2,0:T(8,128)(2,1)} %bitcast.69, f32[32,4,2,1024]{3,2,1,0:T(2,128)S(1)} %get-tuple-element.176, f32[32,4,2]{2,1,0:T(4,128)S(1)} %get-tuple-element.175), kind=kOutput, calls=%fused_computation.33 | convolution fusion | flops 34078720 | bytes 17892352 | tf_op jit(solution)/shard_map/bkgp,bpkd->bkgd/dot_general | solution.py:79
  386.0 32.9 %all-gather.5 = f32[256,4,2,64]{3,1,2,0:T(4,128)S(1)} all-gather(f32[32,4,2,64]{3,1,2,0:T(4,128)S(1)} %copy.114), channel_id=7, replica_groups=mesh['kv'=8,'tp'=4] {'kv'}, dimensions={0}, use_global_device_ids=true | all-gather | bytes 589824 | tf_op jit(solution)/shard_map/all_gather | solution.py:14
  419.8 32.1 %all-gather.2 = f32[256,4,2,64]{3,1,2,0:T(4,128)S(1)} all-gather(f32[32,4,2,64]{3,1,2,0:T(4,128)S(1)} %copy.111), channel_id=4, replica_groups=mesh['kv'=8,'tp'=4] {'kv'}, dimensions={0}, use_global_device_ids=true | all-gather | bytes 589824 | tf_op jit(solution)/shard_map/all_gather | solution.py:14
  453.3 1.1 copy.125
  454.5 1.1 copy.128
  455.5 1.0 copy.124
  456.5 1.0 copy.121
  457.6 11.1 %while.20 = (s32[]{:T(128)}, f32[32,4,2]{0,2,1:T(2,128)S(1)}, f32[32,4,2]{0,2,1:T(2,128)S(1)}, f32[32,4,2,64]{3,2,1,0:T(2,128)S(1)}, f32[32,4,2]{0,2,1:T(2,128)S...) while((s32[]{:T(128)}, f32[32,4,2]{0,2,1:T(2,128)S(1)}, ...), condition=%wide.region_13.14_spmd, body=%wide.region_12.13_spmd.sunk | while | flops 101378 | bytes 684189 | solution.py:17
  458.2 1.0 fusion.73
  459.7 1.0 fusion.73
  461.3 1.0 fusion.73
  462.9 1.0 fusion.73
  464.5 1.0 fusion.73
  466.1 1.0 fusion.73
  467.6 1.0 fusion.73
  470.0 0.8 fusion.56
  470.9 31.2 %all-reduce.13.cloned.1.call-done = f32[32,512]{1,0:T(8,128)} async-done(((f32[32,512]{1,0:T(8,128)}), f32[32,512]{1,0:T(8,128)}) %all-reduce.13.cloned.1.call-update) | async-done | bytes 65552 | tf_op jit(solution)/shard_map/psum | solution.py:103
  502.1 1.0 multiply_reduce_fusion.1
  503.1 3.1 fusion.46
  506.2 3.3 fusion.47
  509.6 21.5 %psum.85 = f32[32,1]{0,1:T(1,128)S(1)} all-reduce(f32[32,1]{0,1:T(1,128)S(1)} %bitcast.78), channel_id=1, replica_groups=mesh['kv'=8,'tp'=4] {'kv'}, use_global_device_ids=true, to_apply=%region_18.19 | all-reduce | flops 32 | bytes 256 | tf_op jit(solution)/shard_map/psum | solution.py:22
  531.1 53.4 %all-reduce.17.cloned.1.call-done = (f32[32,2816]{1,0:T(8,128)}, f32[32,2816]{1,0:T(8,128)}) async-done(((f32[32,2816]{1,0:T(8,128)}, f32[32,2816]{1,0:T(8,128)}), (f32[32,2816]{1,0:T(8,128)}, f32[32,2816]{1,0:T(8,128)})) %all-reduce.17.cloned.1.call-update) | async-done | bytes 720912 | tf_op jit(solution)/shard_map/psum | solution.py:31
  584.5 3.3 fusion.29
  587.8 30.8 %all-reduce.15.cloned.1.call-done = f32[32,512]{1,0:T(8,128)} async-done(((f32[32,512]{1,0:T(8,128)}), f32[32,512]{1,0:T(8,128)}) %all-reduce.15.cloned.1.call-update) | async-done | bytes 65552 | tf_op jit(solution)/shard_map/psum | solution.py:35
  618.7 1.3 fusion.45
  (146 shorter events, 10.3 us)
Async XLA Ops:
  6.5 6.5 %copy-start = (bf16[512,2816]{1,0:T(8,128)(2,1)S(1)}, bf16[512,2816]{1,0:T(8,128)(2,1)}, u32[]{:S(2)}) copy-start(bf16[512,2816]{1,0:T(8,128)(2,1)} %param.21) | copy-start | bytes 8650756
  6.5 8.5 %copy-start.12 = (f32[512]{0:T(512)S(1)}, f32[512]{0:T(512)}, u32[]{:S(2)}) copy-start(f32[512]{0:T(512)} %param.19) | copy-start | bytes 6148
  6.5 86.6 %all-reduce.19.cloned.1.call-start = ((), (), s32[]{:S(2)}) async-start(), calls=%async_computation.5 | async-start | bytes 1441792 | tf_op jit(solution)/shard_map/psum | solution.py:31
  6.5 8.5 %copy-start.2 = (bf16[512,2816]{1,0:T(8,128)(2,1)S(1)}, bf16[512,2816]{1,0:T(8,128)(2,1)}, u32[]{:S(2)}) copy-start(bf16[512,2816]{1,0:T(8,128)(2,1)} %param.20) | copy-start | bytes 8650756
  15.0 78.1 %copy-start.3 = (bf16[2816,512]{1,0:T(8,128)(2,1)S(1)}, bf16[2816,512]{1,0:T(8,128)(2,1)}, u32[]{:S(2)}) copy-start(bf16[2816,512]{1,0:T(8,128)(2,1)} %param.22) | copy-start | bytes 8650756
  16.4 79.2 %copy-start.16 = (f32[8]{0:T(128)S(1)}, f32[8]{0:T(128)}, u32[]{:S(2)}) copy-start(f32[8]{0:T(128)} %param.27) | copy-start | bytes 100
  16.4 124.3 %all-reduce.9.cloned.1.call-start = ((), (), s32[]{:S(2)}) async-start(), calls=%async_computation | async-start | bytes 131072 | tf_op jit(solution)/shard_map/psum | solution.py:35
  95.5 134.1 %all-reduce.11.cloned.1.call-start = ((), (), s32[]{:S(2)}) async-start(), calls=%async_computation.1 | async-start | bytes 131072 | tf_op jit(solution)/shard_map/psum | solution.py:60
  118.2 43.1 %copy-start.10 = (bf16[512,512]{1,0:T(8,128)(2,1)S(1)}, bf16[512,512]{1,0:T(8,128)(2,1)}, u32[]{:S(2)}) copy-start(bf16[512,512]{1,0:T(8,128)(2,1)} %param.24) | copy-start | bytes 1572868
  118.2 43.1 %copy-start.14 = (f32[512]{0:T(512)S(1)}, f32[512]{0:T(512)}, u32[]{:S(2)}) copy-start(f32[512]{0:T(512)} %param.23) | copy-start | bytes 6148
  163.0 339.1 %all-reduce.13.cloned.1.call-start = ((), (), s32[]{:S(2)}) async-start(), calls=%async_computation.2 | async-start | bytes 131072 | tf_op jit(solution)/shard_map/psum | solution.py:103
  272.9 104.9 %copy-start.4 = (f32[256,4,2]{1,2,0:T(2,128)}, f32[256,4,2]{1,2,0:T(2,128)S(1)}, u32[]{:S(2)}) copy-start(f32[256,4,2]{1,2,0:T(2,128)S(1)} %all-gather.1) | copy-start | bytes 24580
  305.4 72.4 %copy-start.5 = (f32[256,4,2]{1,2,0:T(2,128)}, f32[256,4,2]{1,2,0:T(2,128)S(1)}, u32[]{:S(2)}) copy-start(f32[256,4,2]{1,2,0:T(2,128)S(1)} %all-gather.4) | copy-start | bytes 24580
  336.4 41.4 %copy-start.6 = (f32[256,4,2]{1,2,0:T(2,128)}, f32[256,4,2]{1,2,0:T(2,128)S(1)}, u32[]{:S(2)}) copy-start(f32[256,4,2]{1,2,0:T(2,128)S(1)} %all-gather) | copy-start | bytes 24580
  368.2 9.6 %copy-start.7 = (f32[256,4,2]{1,2,0:T(2,128)}, f32[256,4,2]{1,2,0:T(2,128)S(1)}, u32[]{:S(2)}) copy-start(f32[256,4,2]{1,2,0:T(2,128)S(1)} %all-gather.3) | copy-start | bytes 24580
  377.8 8.2 %copy-start.11 = (f32[32,4,2,64]{3,2,1,0:T(2,128)S(1)}, f32[32,4,2,64]{3,2,1,0:T(2,128)}, u32[]{:S(2)}) copy-start(f32[32,4,2,64]{3,2,1,0:T(2,128)} %fusion.22) | copy-start | bytes 196612
  418.9 33.8 %slice-start = ((f32[256,4,2]{1,2,0:T(2,128)}), f32[32,4,2]{1,2,0:T(2,128)S(1)}, s32[]{:S(2)}) async-start(f32[256,4,2]{1,2,0:T(2,128)} %copy-done.4), calls=%async_computation.6 | async-start | bytes 65536 | tf_op jit(solution)/shard_map/slice | solution.py:15
  418.9 33.9 %slice-start.1 = ((f32[256,4,2]{1,2,0:T(2,128)}), f32[224,4,2]{1,2,0:T(2,128)S(1)}, s32[]{:S(2)}) async-start(f32[256,4,2]{1,2,0:T(2,128)} %copy-done.4), calls=%async_computation.7 | async-start | bytes 458752 | tf_op jit(solution)/shard_map/slice | solution.py:16
  419.5 33.4 %slice-start.2 = ((f32[256,4,2]{1,2,0:T(2,128)}), f32[32,4,2]{1,2,0:T(2,128)S(1)}, s32[]{:S(2)}) async-start(f32[256,4,2]{1,2,0:T(2,128)} %copy-done.5), calls=%async_computation.8 | async-start | bytes 65536 | tf_op jit(solution)/shard_map/slice | solution.py:15
  419.6 33.5 %slice-start.3 = ((f32[256,4,2]{1,2,0:T(2,128)}), f32[224,4,2]{1,2,0:T(2,128)S(1)}, s32[]{:S(2)}) async-start(f32[256,4,2]{1,2,0:T(2,128)} %copy-done.5), calls=%async_computation.9 | async-start | bytes 458752 | tf_op jit(solution)/shard_map/slice | solution.py:16
  419.6 33.6 %slice-start.4 = ((f32[256,4,2]{1,2,0:T(2,128)}), f32[32,4,2]{1,2,0:T(2,128)S(1)}, s32[]{:S(2)}) async-start(f32[256,4,2]{1,2,0:T(2,128)} %copy-done.6), calls=%async_computation.10 | async-start | bytes 65536 | tf_op jit(solution)/shard_map/slice | solution.py:15
  419.6 34.8 %slice-start.5 = ((f32[256,4,2]{1,2,0:T(2,128)}), f32[32,4,2]{1,2,0:T(2,128)S(1)}, s32[]{:S(2)}) async-start(f32[256,4,2]{1,2,0:T(2,128)} %copy-done.7), calls=%async_computation.11 | async-start | bytes 65536 | tf_op jit(solution)/shard_map/slice | solution.py:15
  457.5 12.1 %copy-start.15 = (f32[64]{0:T(128)S(1)}, f32[64]{0:T(128)}, u32[]{:S(2)}) copy-start(f32[64]{0:T(128)} %param.28) | copy-start | bytes 772
  457.5 12.5 %copy-start.9 = (bf16[512,512]{1,0:T(8,128)(2,1)S(1)}, bf16[512,512]{1,0:T(8,128)(2,1)}, u32[]{:S(2)}) copy-start(bf16[512,512]{1,0:T(8,128)(2,1)} %param.29) | copy-start | bytes 1572868
  457.5 44.6 %copy-start.8 = (f32[32,512]{1,0:T(8,128)S(1)}, f32[32,512]{1,0:T(8,128)}, u32[]{:S(2)}) copy-start(f32[32,512]{1,0:T(8,128)} %all-reduce.9.cloned.1.call-done) | copy-start | bytes 196612
  457.6 45.5 %copy-start.13 = (f32[512]{0:T(512)S(1)}, f32[512]{0:T(512)}, u32[]{:S(2)}) copy-start(f32[512]{0:T(512)} %param.30) | copy-start | bytes 6148
  470.9 113.6 %all-reduce.17.cloned.1.call-start = ((), (), s32[]{:S(2)}) async-start(), calls=%async_computation.4 | async-start | bytes 1441792 | tf_op jit(solution)/shard_map/psum | solution.py:31
  506.2 113.8 %copy-start.1 = (bf16[512,2816]{1,0:T(8,128)(2,1)S(1)}, bf16[512,2816]{1,0:T(8,128)(2,1)}, u32[]{:S(2)}) copy-start(bf16[512,2816]{1,0:T(8,128)(2,1)} %param.21) | copy-start | bytes 8650756
  509.6 109.1 %all-reduce.15.cloned.1.call-start = ((), (), s32[]{:S(2)}) async-start(), calls=%async_computation.3 | async-start | bytes 131072 | tf_op jit(solution)/shard_map/psum | solution.py:35
Sparse Core Ops, SparseCore 0:
  16.5 76.5 all-reduce.18
  95.6 30.6 all-reduce.8
  163.1 66.4 all-reduce.10
  471.0 31.0 all-reduce.12
  509.7 74.7 all-reduce.16
  588.0 30.6 all-reduce.14
where the time goes:
time: 629 us; the launch traced here: 627 us
  blocking collectives  259 us (41%)
  waiting for transfers between devices  236 us (38%)
  local copies, waits for them, and re-layouts  58.6 us (9%)
  matrix products  44.7 us (7%)
  other arithmetic  14.3 us (2%)
  between operations  13.7 us (2%)
    all_gather x6, blocking collectives, merged(): pieces = jax.tree.map(lambda part: lax.all_gather(part, axis), value)  189 us
    psum x2, waiting for transfers between devices, channel_mixer(): gate_sum, up_sum = lax.psum((part_gate, part_up), 'kv')  107 us
    psum x1, waiting for transfers between devices, attention_mix(): queries = lax.psum(part_query, 'kv')  66.6 us
    psum x3, blocking collectives, norm_total(): return lax.psum(squares, 'kv')  63.8 us
    unnamed x36, local copies, waits for them, and re-layouts  45.2 us
    psum x1, waiting for transfers between devices, attention_mix(): return lax.psum(partial_value, 'tp')  31.2 us
    psum x2, waiting for transfers between devices, channel_mixer(): return lax.psum(partial_value, 'tp')  30.8 us
    dot_general x2, matrix products, partial_map(): jnp.einsum('bkgp,bpkd->bkgd', exp_terms.astype(jnp.bfloat16), stored, pre...  16.9 us
  transfers between devices with their start and end apart: 6, of which 5 were waited for; matrix products, arithmetic and copies ran while one was open for 7% of the time, Pallas kernels for 0%

commit v1 on v0

--- a/solution.py
+++ b/solution.py
@@ -57,7 +57,9 @@
     scaled = (residual * mix_gain).astype(jnp.bfloat16)
     part_query = jnp.dot(scaled, w_query, preferred_element_type=jnp.float32)
     row_total = norm_total(squares)
-    queries = lax.psum(part_query, "kv")
+    queries = part_query
+    for hop in (1, 2, 4):
+        queries = queries + lax.ppermute(queries, "kv", [(dev, dev ^ hop) for dev in range(8)])
     queries = (queries * lax.rsqrt(row_total / D + EPS)).astype(jnp.bfloat16)
     batch_rows = queries.shape[0]
     kv_local = key_cache.shape[2] // HEAD

time: 629 us -> 596 us (0.948)
  waiting for transfers between devices: 236 us -> 202 us
    psum x1 -> x0, waiting for transfers between devices: 66.6 us -> none  [attention_mix(): queries = lax.psum(part_query, 'kv')]
    psum x2, waiting for transfers between devices: 30.8 us -> 61.6 us  [channel_mixer(): return lax.psum(partial_value, 'tp')]
    unnamed x36 -> x38, local copies, waits for them, and re-layouts: 45.2 us -> 45.1 us
  transfers between devices with their start and end apart: 6 -> 8, of which waited for: 5 -> 6; matrix products, arithmetic and copies ran while one was open for 7% -> 8% of each run, Pallas kernels for 0% -> 0%
where the time goes in v1:
time: 596 us; the launch traced here: 594 us
  blocking collectives  260 us (44%)
  waiting for transfers between devices  202 us (34%)
  local copies, waits for them, and re-layouts  58.5 us (10%)
  matrix products  44.2 us (7%)
  between operations  13.4 us (2%)
  other arithmetic  12.6 us (2%)
    all_gather x6, blocking collectives, merged(): pieces = jax.tree.map(lambda part: lax.all_gather(part, axis), value)  190 us
    psum x2, waiting for transfers between devices, channel_mixer(): gate_sum, up_sum = lax.psum((part_gate, part_up), 'kv')  107 us
    psum x3, blocking collectives, norm_total(): return lax.psum(squares, 'kv')  63.8 us
    psum x2, waiting for transfers between devices, channel_mixer(): return lax.psum(partial_value, 'tp')  61.6 us
    unnamed x38, local copies, waits for them, and re-layouts  45.1 us
    psum x1, waiting for transfers between devices, attention_mix(): return lax.psum(partial_value, 'tp')  27.9 us
    dot_general x2, matrix products, partial_map(): jnp.einsum('bkgp,bpkd->bkgd', exp_terms.astype(jnp.bfloat16), stored, pre...  16.9 us
  transfers between devices with their start and end apart: 8, of which 6 were waited for; matrix products, arithmetic and copies ran while one was open for 8% of the time, Pallas kernels for 0%

profile of v1, /device:TPU:0, one launch (start us, length us, event | category | flops | bytes accessed | tf_op | source)
XLA Modules:
  0.0 594.1 jit_solution(11337261283790991541)
XLA Ops:
  6.5 6.5 %all_gather.39 = bf16[32,512]{1,0:T(8,128)(2,1)S(1)} all-gather(bf16[32,128]{1,0:T(8,128)(2,1)} %param.18), channel_id=1, replica_groups=mesh['kv'=8,'tp'=4] {'tp'}, dimensions={1}, use_global_device_ids=true | all-gather | bytes 40960 | tf_op jit(solution)/shard_map/all_gather | solution.py:126
  13.0 2.0 fusion.40
  15.1 1.3 fusion.42
  16.6 22.7 %psum.71 = f32[32,1]{0,1:T(1,128)S(1)} all-reduce(f32[32,1]{0,1:T(1,128)S(1)} %bitcast.79), channel_id=1, replica_groups=mesh['kv'=8,'tp'=4] {'kv'}, use_global_device_ids=true, to_apply=%region_2.0 | all-reduce | flops 32 | bytes 256 | tf_op jit(solution)/shard_map/psum | solution.py:22
  39.3 53.8 %all-reduce.16.cloned.1.call-done = (f32[32,2816]{1,0:T(8,128)}, f32[32,2816]{1,0:T(8,128)}) async-done(((f32[32,2816]{1,0:T(8,128)}, f32[32,2816]{1,0:T(8,128)}), (f32[32,2816]{1,0:T(8,128)}, f32[32,2816]{1,0:T(8,128)})) %all-reduce.16.cloned.1.call-update) | async-done | bytes 720912 | tf_op jit(solution)/shard_map/psum | solution.py:31
  93.1 2.4 fusion.28
  95.6 30.8 %all-reduce.8.cloned.1.call-done = f32[32,512]{1,0:T(8,128)} async-done(((f32[32,512]{1,0:T(8,128)}), f32[32,512]{1,0:T(8,128)}) %all-reduce.8.cloned.1.call-update) | async-done | bytes 65552 | tf_op jit(solution)/shard_map/psum | solution.py:35
  126.4 1.0 fusion.38
  127.4 1.5 collective-permute-start
  129.0 22.5 %copy.107 = bf16[32,1024,256]{1,2,0:T(8,128)(2,1)} copy(bf16[32,1024,256]{2,1,0:T(8,128)(2,1)} %param.25) | data formatting | bytes 33554432 | tf_op args[7]
  151.5 22.5 %copy.110 = bf16[32,1024,256]{1,2,0:T(8,128)(2,1)} copy(bf16[32,1024,256]{2,1,0:T(8,128)(2,1)} %param.26) | data formatting | bytes 33554432 | tf_op args[8]
  174.0 1.6 collective-permute-start.1
  175.7 19.6 %psum.74 = f32[32,1]{0,1:T(1,128)S(1)} all-reduce(f32[32,1]{0,1:T(1,128)S(1)} %bitcast.80), channel_id=1, replica_groups=mesh['kv'=8,'tp'=4] {'kv'}, use_global_device_ids=true, to_apply=%region_6.7 | all-reduce | flops 32 | bytes 256 | tf_op jit(solution)/shard_map/psum | solution.py:22
  195.4 5.1 collective-permute-done.2
  200.7 4.9 fusion.55
  205.6 4.9 fusion.54
  210.8 0.9 fusion.19
  212.1 30.8 %all-gather.1 = f32[256,4,2]{1,2,0:T(2,128)S(1)} all-gather(f32[32,4,2]{1,2,0:T(2,128)S(1)} %copy.109), channel_id=3, replica_groups=mesh['kv'=8,'tp'=4] {'kv'}, dimensions={0}, use_global_device_ids=true | all-gather | bytes 9216 | tf_op jit(solution)/shard_map/all_gather | solution.py:14
  243.2 1.0 fusion.21
  244.5 30.9 %all-gather.4 = f32[256,4,2]{1,2,0:T(2,128)S(1)} all-gather(f32[32,4,2]{1,2,0:T(2,128)S(1)} %copy.113), channel_id=6, replica_groups=mesh['kv'=8,'tp'=4] {'kv'}, dimensions={0}, use_global_device_ids=true | all-gather | bytes 9216 | tf_op jit(solution)/shard_map/all_gather | solution.py:14
  275.3 30.7 %all-gather = f32[256,4,2]{1,2,0:T(2,128)S(1)} all-gather(f32[32,4,2]{1,2,0:T(2,128)S(1)} %copy.108), channel_id=2, replica_groups=mesh['kv'=8,'tp'=4] {'kv'}, dimensions={0}, use_global_device_ids=true | all-gather | bytes 9216 | tf_op jit(solution)/shard_map/all_gather | solution.py:14
  306.8 31.3 %all-gather.3 = f32[256,4,2]{1,2,0:T(2,128)S(1)} all-gather(f32[32,4,2]{1,2,0:T(2,128)S(1)} %copy.112), channel_id=5, replica_groups=mesh['kv'=8,'tp'=4] {'kv'}, dimensions={0}, use_global_device_ids=true | all-gather | bytes 9216 | tf_op jit(solution)/shard_map/all_gather | solution.py:14
  338.8 8.8 %fusion.22 = f32[32,4,2,64]{3,2,1,0:T(2,128)} fusion(bf16[32,1024,4,64]{1,3,2,0:T(8,128)(2,1)} %bitcast.68, f32[32,4,2,1024]{3,2,1,0:T(2,128)S(1)} %get-tuple-element.178, f32[32,4,2]{2,1,0:T(4,128)S(1)} %get-tuple-element.177), kind=kOutput, calls=%fused_computation.32 | convolution fusion | flops 34078720 | bytes 17892352 | tf_op jit(solution)/shard_map/bkgp,bpkd->bkgd/dot_general | solution.py:81
  347.6 8.2 %fusion.24 = f32[32,4,2,64]{3,2,1,0:T(2,128)S(1)} fusion(bf16[32,1024,4,64]{1,3,2,0:T(8,128)(2,1)} %bitcast.69, f32[32,4,2,1024]{3,2,1,0:T(2,128)S(1)} %get-tuple-element.176, f32[32,4,2]{2,1,0:T(4,128)S(1)} %get-tuple-element.175), kind=kOutput, calls=%fused_computation.33 | convolution fusion | flops 34078720 | bytes 17892352 | tf_op jit(solution)/shard_map/bkgp,bpkd->bkgd/dot_general | solution.py:81
  355.8 33.5 %all-gather.5 = f32[256,4,2,64]{3,1,2,0:T(4,128)S(1)} all-gather(f32[32,4,2,64]{3,1,2,0:T(4,128)S(1)} %copy.114), channel_id=7, replica_groups=mesh['kv'=8,'tp'=4] {'kv'}, dimensions={0}, use_global_device_ids=true | all-gather | bytes 589824 | tf_op jit(solution)/shard_map/all_gather | solution.py:14
  390.2 32.6 %all-gather.2 = f32[256,4,2,64]{3,1,2,0:T(4,128)S(1)} all-gather(f32[32,4,2,64]{3,1,2,0:T(4,128)S(1)} %copy.111), channel_id=4, replica_groups=mesh['kv'=8,'tp'=4] {'kv'}, dimensions={0}, use_global_device_ids=true | all-gather | bytes 589824 | tf_op jit(solution)/shard_map/all_gather | solution.py:14
  424.2 1.1 copy.125
  425.4 1.1 copy.128
  426.5 1.0 copy.124
  427.5 1.0 copy.121
  428.5 11.1 %while.20 = (s32[]{:T(128)}, f32[32,4,2]{0,2,1:T(2,128)S(1)}, f32[32,4,2]{0,2,1:T(2,128)S(1)}, f32[32,4,2,64]{3,2,1,0:T(2,128)S(1)}, f32[32,4,2]{0,2,1:T(2,128)S...) while((s32[]{:T(128)}, f32[32,4,2]{0,2,1:T(2,128)S(1)}, ...), condition=%wide.region_12.13_spmd, body=%wide.region_11.12_spmd.sunk | while | flops 101378 | bytes 684189 | solution.py:17
  429.1 1.0 fusion.73
  430.7 1.0 fusion.73
  432.3 1.0 fusion.73
  433.8 1.0 fusion.73
  435.4 1.0 fusion.73
  437.0 1.0 fusion.73
  438.6 1.0 fusion.73
  440.9 0.8 fusion.56
  441.8 27.9 %all-reduce.10.cloned.1.call-done = f32[32,512]{1,0:T(8,128)} async-done(((f32[32,512]{1,0:T(8,128)}), f32[32,512]{1,0:T(8,128)}) %all-reduce.10.cloned.1.call-update) | async-done | bytes 65552 | tf_op jit(solution)/shard_map/psum | solution.py:105
  469.8 1.0 multiply_reduce_fusion.1
  470.8 3.2 fusion.46
  473.9 3.3 fusion.47
  477.3 21.6 %psum.77 = f32[32,1]{0,1:T(1,128)S(1)} all-reduce(f32[32,1]{0,1:T(1,128)S(1)} %bitcast.78), channel_id=1, replica_groups=mesh['kv'=8,'tp'=4] {'kv'}, use_global_device_ids=true, to_apply=%region_17.18 | all-reduce | flops 32 | bytes 256 | tf_op jit(solution)/shard_map/psum | solution.py:22
  498.9 53.2 %all-reduce.14.cloned.1.call-done = (f32[32,2816]{1,0:T(8,128)}, f32[32,2816]{1,0:T(8,128)}) async-done(((f32[32,2816]{1,0:T(8,128)}, f32[32,2816]{1,0:T(8,128)}), (f32[32,2816]{1,0:T(8,128)}, f32[32,2816]{1,0:T(8,128)})) %all-reduce.14.cloned.1.call-update) | async-done | bytes 720912 | tf_op jit(solution)/shard_map/psum | solution.py:31
  552.1 3.3 fusion.29
  555.5 30.8 %all-reduce.12.cloned.1.call-done = f32[32,512]{1,0:T(8,128)} async-done(((f32[32,512]{1,0:T(8,128)}), f32[32,512]{1,0:T(8,128)}) %all-reduce.12.cloned.1.call-update) | async-done | bytes 65552 | tf_op jit(solution)/shard_map/psum | solution.py:35
  586.3 1.3 fusion.45
  (153 shorter events, 11.3 us)
Async XLA Ops:
  6.5 6.5 %copy-start = (bf16[512,2816]{1,0:T(8,128)(2,1)S(1)}, bf16[512,2816]{1,0:T(8,128)(2,1)}, u32[]{:S(2)}) copy-start(bf16[512,2816]{1,0:T(8,128)(2,1)} %param.21) | copy-start | bytes 8650756
  6.5 8.5 %copy-start.13 = (f32[512]{0:T(512)S(1)}, f32[512]{0:T(512)}, u32[]{:S(2)}) copy-start(f32[512]{0:T(512)} %param.19) | copy-start | bytes 6148
  6.5 86.6 %all-reduce.16.cloned.1.call-start = ((), (), s32[]{:S(2)}) async-start(), calls=%async_computation.4 | async-start | bytes 1441792 | tf_op jit(solution)/shard_map/psum | solution.py:31
  6.5 8.5 %copy-start.2 = (bf16[512,2816]{1,0:T(8,128)(2,1)S(1)}, bf16[512,2816]{1,0:T(8,128)(2,1)}, u32[]{:S(2)}) copy-start(bf16[512,2816]{1,0:T(8,128)(2,1)} %param.20) | copy-start | bytes 8650756
  15.1 78.1 %copy-start.3 = (bf16[2816,512]{1,0:T(8,128)(2,1)S(1)}, bf16[2816,512]{1,0:T(8,128)(2,1)}, u32[]{:S(2)}) copy-start(bf16[2816,512]{1,0:T(8,128)(2,1)} %param.22) | copy-start | bytes 8650756
  16.4 109.9 %copy-start.11 = (bf16[512,512]{1,0:T(8,128)(2,1)S(1)}, bf16[512,512]{1,0:T(8,128)(2,1)}, u32[]{:S(2)}) copy-start(bf16[512,512]{1,0:T(8,128)(2,1)} %param.24) | copy-start | bytes 1572868
  16.4 109.9 %copy-start.15 = (f32[512]{0:T(512)S(1)}, f32[512]{0:T(512)}, u32[]{:S(2)}) copy-start(f32[512]{0:T(512)} %param.23) | copy-start | bytes 6148
  16.4 112.4 %copy-start.17 = (f32[8]{0:T(128)S(1)}, f32[8]{0:T(128)}, u32[]{:S(2)}) copy-start(f32[8]{0:T(128)} %param.27) | copy-start | bytes 100
  16.5 109.9 %all-reduce.8.cloned.1.call-start = ((), (), s32[]{:S(2)}) async-start(), calls=%async_computation | async-start | bytes 131072 | tf_op jit(solution)/shard_map/psum | solution.py:35
  95.5 374.2 %all-reduce.10.cloned.1.call-start = ((), (), s32[]{:S(2)}) async-start(), calls=%async_computation.1 | async-start | bytes 131072 | tf_op jit(solution)/shard_map/psum | solution.py:105
  127.4 46.6 %collective-permute-start = (f32[32,512]{1,0:T(8,128)S(1)}, f32[32,512]{1,0:T(8,128)S(1)}, u32[]{:S(2)}, u32[]{:S(2)}) collective-permute-start(f32[32,512]{1,0:T(8,128)S(1)} %fusion.38), channel_id=1, source_target_pairs={{0,4},{4,0},{8,12},{12,8},{16,20},{20,16},{24,28},{28,24},{1,5},{5... | collective-permute-start | bytes 196616 | tf_op jit(solution)/shard_map/ppermute | solution.py:62
  151.5 24.1 %copy-start.8 = (f32[32,512]{1,0:T(8,128)S(1)}, f32[32,512]{1,0:T(8,128)}, u32[]{:S(2)}) copy-start(f32[32,512]{1,0:T(8,128)} %all-reduce.8.cloned.1.call-done) | copy-start | bytes 196612
  174.0 21.3 %collective-permute-start.1 = (f32[32,512]{1,0:T(8,128)S(1)}, f32[32,512]{1,0:T(8,128)S(1)}, u32[]{:S(2)}, u32[]{:S(2)}) collective-permute-start(f32[32,512]{1,0:T(8,128)S(1)} %add.86), channel_id=1, source_target_pairs={{0,8},{4,12},{8,0},{12,4},{16,24},{20,28},{24,16},{28,20},{1,9},{5... | collective-permute-start | bytes 196616 | tf_op jit(solution)/shard_map/ppermute | solution.py:62
  195.3 5.2 collective-permute-start.2
  242.9 104.7 %copy-start.4 = (f32[256,4,2]{1,2,0:T(2,128)}, f32[256,4,2]{1,2,0:T(2,128)S(1)}, u32[]{:S(2)}) copy-start(f32[256,4,2]{1,2,0:T(2,128)S(1)} %all-gather.1) | copy-start | bytes 24580
  275.3 72.3 %copy-start.5 = (f32[256,4,2]{1,2,0:T(2,128)}, f32[256,4,2]{1,2,0:T(2,128)S(1)}, u32[]{:S(2)}) copy-start(f32[256,4,2]{1,2,0:T(2,128)S(1)} %all-gather.4) | copy-start | bytes 24580
  306.1 41.5 %copy-start.6 = (f32[256,4,2]{1,2,0:T(2,128)}, f32[256,4,2]{1,2,0:T(2,128)S(1)}, u32[]{:S(2)}) copy-start(f32[256,4,2]{1,2,0:T(2,128)S(1)} %all-gather) | copy-start | bytes 24580
  338.1 9.5 %copy-start.7 = (f32[256,4,2]{1,2,0:T(2,128)}, f32[256,4,2]{1,2,0:T(2,128)S(1)}, u32[]{:S(2)}) copy-start(f32[256,4,2]{1,2,0:T(2,128)S(1)} %all-gather.3) | copy-start | bytes 24580
  347.6 8.2 %copy-start.12 = (f32[32,4,2,64]{3,2,1,0:T(2,128)S(1)}, f32[32,4,2,64]{3,2,1,0:T(2,128)}, u32[]{:S(2)}) copy-start(f32[32,4,2,64]{3,2,1,0:T(2,128)} %fusion.22) | copy-start | bytes 196612
  389.3 34.3 %slice-start = ((f32[256,4,2]{1,2,0:T(2,128)}), f32[32,4,2]{1,2,0:T(2,128)S(1)}, s32[]{:S(2)}) async-start(f32[256,4,2]{1,2,0:T(2,128)} %copy-done.4), calls=%async_computation.5 | async-start | bytes 65536 | tf_op jit(solution)/shard_map/slice | solution.py:15
  389.3 34.4 %slice-start.1 = ((f32[256,4,2]{1,2,0:T(2,128)}), f32[224,4,2]{1,2,0:T(2,128)S(1)}, s32[]{:S(2)}) async-start(f32[256,4,2]{1,2,0:T(2,128)} %copy-done.4), calls=%async_computation.6 | async-start | bytes 458752 | tf_op jit(solution)/shard_map/slice | solution.py:16
  390.0 33.9 %slice-start.2 = ((f32[256,4,2]{1,2,0:T(2,128)}), f32[32,4,2]{1,2,0:T(2,128)S(1)}, s32[]{:S(2)}) async-start(f32[256,4,2]{1,2,0:T(2,128)} %copy-done.5), calls=%async_computation.7 | async-start | bytes 65536 | tf_op jit(solution)/shard_map/slice | solution.py:15
  390.0 34.0 %slice-start.3 = ((f32[256,4,2]{1,2,0:T(2,128)}), f32[224,4,2]{1,2,0:T(2,128)S(1)}, s32[]{:S(2)}) async-start(f32[256,4,2]{1,2,0:T(2,128)} %copy-done.5), calls=%async_computation.8 | async-start | bytes 458752 | tf_op jit(solution)/shard_map/slice | solution.py:16
  390.0 34.1 %slice-start.4 = ((f32[256,4,2]{1,2,0:T(2,128)}), f32[32,4,2]{1,2,0:T(2,128)S(1)}, s32[]{:S(2)}) async-start(f32[256,4,2]{1,2,0:T(2,128)} %copy-done.6), calls=%async_computation.9 | async-start | bytes 65536 | tf_op jit(solution)/shard_map/slice | solution.py:15
  390.0 35.3 %slice-start.5 = ((f32[256,4,2]{1,2,0:T(2,128)}), f32[32,4,2]{1,2,0:T(2,128)S(1)}, s32[]{:S(2)}) async-start(f32[256,4,2]{1,2,0:T(2,128)} %copy-done.7), calls=%async_computation.10 | async-start | bytes 65536 | tf_op jit(solution)/shard_map/slice | solution.py:15
  428.5 12.1 %copy-start.16 = (f32[64]{0:T(128)S(1)}, f32[64]{0:T(128)}, u32[]{:S(2)}) copy-start(f32[64]{0:T(128)} %param.28) | copy-start | bytes 772
  428.5 12.5 %copy-start.10 = (bf16[512,512]{1,0:T(8,128)(2,1)S(1)}, bf16[512,512]{1,0:T(8,128)(2,1)}, u32[]{:S(2)}) copy-start(bf16[512,512]{1,0:T(8,128)(2,1)} %param.29) | copy-start | bytes 1572868
  428.5 41.3 %copy-start.9 = (f32[32,512]{1,0:T(8,128)S(1)}, f32[32,512]{1,0:T(8,128)}, u32[]{:S(2)}) copy-start(f32[32,512]{1,0:T(8,128)} %all-reduce.8.cloned.1.call-done) | copy-start | bytes 196612
  428.5 42.3 %copy-start.14 = (f32[512]{0:T(512)S(1)}, f32[512]{0:T(512)}, u32[]{:S(2)}) copy-start(f32[512]{0:T(512)} %param.30) | copy-start | bytes 6148
  441.8 110.3 %all-reduce.14.cloned.1.call-start = ((), (), s32[]{:S(2)}) async-start(), calls=%async_computation.3 | async-start | bytes 1441792 | tf_op jit(solution)/shard_map/psum | solution.py:31
  473.9 113.7 %copy-start.1 = (bf16[512,2816]{1,0:T(8,128)(2,1)S(1)}, bf16[512,2816]{1,0:T(8,128)(2,1)}, u32[]{:S(2)}) copy-start(bf16[512,2816]{1,0:T(8,128)(2,1)} %param.21) | copy-start | bytes 8650756
  477.3 109.0 %all-reduce.12.cloned.1.call-start = ((), (), s32[]{:S(2)}) async-start(), calls=%async_computation.2 | async-start | bytes 131072 | tf_op jit(solution)/shard_map/psum | solution.py:35
Sparse Core Ops, SparseCore 0:
  16.6 76.5 all-reduce.15
  95.7 30.6 all-reduce.7
  441.9 27.8 all-reduce.9
  477.4 74.6 all-reduce.13
  555.6 30.6 all-reduce.11
